TPU v7x, 32 devices: a whole 2x2x4 slice. The times are simulated.
32 devices in a mesh: dp: 4 (over y, x), kv: 4 (over z), tp: 2 (over core).
Axes of the slice: x: 2, y: 2, z: 4, core: 2. Of those that a mesh axis runs over, the one named last changes fastest.
Arguments:
- tokens: bfloat16 [64, 4096], P('dp', 'kv'), may hold values from -51 to 51
- norm_gain: float32 [4096], P('kv'), may hold values from 0.1 to 1.9
- w_query: bfloat16 [4096, 2048], P('kv', 'tp'), may hold values from -0.09375 to 0.09375
- lambda_head: float32 [16], P('tp'), may hold values from 0.3 to 0.8
- head_gain: float32 [128], replicated, may hold values from 0.1 to 1.9
- w_out: bfloat16 [2048, 4096], P('tp', 'kv'), may hold values from -0.125 to 0.125
- rotated_key_cache: bfloat16 [64, 1024, 128], P('dp', 'kv'), may hold values from -540 to 540, as said below
- value_cache: bfloat16 [64, 1024, 128], P('dp', 'kv'), may hold values from -6 to 6
- lengths: int32 [64], P('dp'), may hold values from 256 to 1024
Outputs:
- mixed: bfloat16 [64, 4096], P('dp', ('kv', 'tp'))
Inputs may be any that keep to these rules, and one draw needn't show every extreme that they name: `rotated_key_cache`: keys have an order-one typical size. The new token is the last filled position, lengths - 1.
All inputs are finite; a program needn't handle non-finite values.
Results may differ from a plain program's by a relative error of at most 0.0112.
Values may be sent and summed in bfloat16 or wider, within the bound.
No kernel may reach another device: no remote copies, remote signals or barrier semaphores. Data moves between devices by JAX's collectives and lax.ppermute only.
A program may use at most 64 MiB of HBM per device.

v0:
```python
import jax
import jax.numpy as jnp
from jax import lax
from jax.sharding import PartitionSpec as P

D = 4096
HEAD_FEATURES = 64
VALUE_DIM = 128
EPS = 1e-05


def combined_all(part, axis, combine):
    gathered = jax.tree.map(lambda a: lax.all_gather(a, axis), part)

    def take(source):
        return jax.tree.map(lambda a: lax.dynamic_index_in_dim(a, source, 0, False), gathered)

    return lax.fori_loop(
        1, lax.axis_size(axis), lambda source, state: combine(state, take(source)), take(0)
    )


def rotate_query(query, position):
    half_dim = query.shape[-1] // 2
    frequency = 1.0 / 10000.0 ** (jnp.arange(half_dim, dtype=jnp.float32) / half_dim)
    angles = position[:, None] * frequency[None, :]
    cosine_table = jnp.concatenate([jnp.cos(angles), jnp.cos(angles)], -1)[:, None, None, :]
    sine_table = jnp.concatenate([jnp.sin(angles), jnp.sin(angles)], -1)[:, None, None, :]
    first_half = query[..., :half_dim]
    second_half = query[..., half_dim:]
    turned = jnp.concatenate([-second_half, first_half], -1)
    return query * cosine_table + turned * sine_table


def finish(numerators, totals, lambdas, head_gain):
    averaged = numerators / totals[..., None]
    head_result = averaged[..., 0, :] - lambdas[..., None] * averaged[..., 1, :]
    factor = lax.rsqrt(jnp.mean(head_result * head_result, -1, keepdims=True) + EPS)
    return (head_result * factor * head_gain).astype(jnp.bfloat16)


def combine_blocks(earlier, later):
    top = jnp.maximum(earlier[0], later[0])
    first_factor = jnp.exp(earlier[0] - top)
    second_factor = jnp.exp(later[0] - top)
    totals = earlier[1] * first_factor + later[1] * second_factor
    numerators = earlier[2] * first_factor[..., None] + later[2] * second_factor[..., None]
    return (top, totals, numerators)


def on_device(
    tokens,
    norm_gain,
    w_query,
    lambda_head,
    head_gain,
    w_out,
    rotated_key_cache,
    value_cache,
    lengths,
):
    seq_count = tokens.shape[0]
    head_count = lambda_head.shape[0]
    pos_count = rotated_key_cache.shape[1]
    widened = tokens.astype(jnp.float32)
    squares = jnp.sum(widened * widened, -1)
    scaled_in = (widened * norm_gain).astype(jnp.bfloat16)
    partial_query = jnp.dot(scaled_in, w_query, preferred_element_type=jnp.float32)
    squares = lax.psum(squares, "kv")
    raw_query = lax.psum(partial_query, "kv")
    scale_rows = lax.rsqrt(squares / D + EPS)
    shaped = (raw_query * scale_rows[:, None]).reshape(seq_count, head_count, 2, HEAD_FEATURES)
    query = rotate_query(shaped, (lengths - 1).astype(jnp.float32))
    keys = rotated_key_cache.reshape(seq_count, pos_count, 2, HEAD_FEATURES)
    score_rows = jnp.einsum(
        "bhmd,bpmd->bhmp",
        query,
        keys,
        preferred_element_type=jnp.float32,
        precision=lax.Precision.HIGHEST,
    ) * HEAD_FEATURES ** (-0.5)
    position_list = lax.axis_index("kv") * pos_count + jnp.arange(pos_count, dtype=jnp.int32)
    valid = (position_list[None, :] < lengths[:, None])[:, None, None, :]
    masked = jnp.where(valid, score_rows, -1e30)
    maxima = jnp.max(masked, -1)
    weights = jnp.where(valid, jnp.exp(masked - maxima[..., None]), 0.0)
    totals = jnp.sum(weights, -1)
    numerators = jnp.einsum(
        "bhmp,bpv->bhmv",
        weights.astype(jnp.bfloat16),
        value_cache,
        preferred_element_type=jnp.float32,
    )
    merged = combined_all((maxima, totals, numerators), "kv", combine_blocks)
    normed = finish(merged[2], merged[1], lambda_head[None, :], head_gain).reshape(
        seq_count, head_count * VALUE_DIM
    )
    projected = jnp.dot(normed, w_out, preferred_element_type=jnp.float32)
    return lax.psum_scatter(projected, "tp", scatter_dimension=1, tiled=True).astype(jnp.bfloat16)


def solution(mesh):
    in_specs = (
        P("dp", "kv"),
        P("kv"),
        P("kv", "tp"),
        P("tp"),
        P(),
        P("tp", "kv"),
        P("dp", "kv", None),
        P("dp", "kv", None),
        P("dp"),
    )
    out_specs = P("dp", ("kv", "tp"))
    return jax.shard_map(
        on_device, mesh=mesh, in_specs=in_specs, out_specs=out_specs, check_vma=False
    )
```

profile of v0, /device:TPU:0, one launch (start us, length us, event | category | flops | bytes accessed | tf_op | source)
XLA Modules:
  0.0 114.8 jit_solution(7172652897911853085)
XLA Ops:
  6.5 0.0 copy-start
  6.5 0.0 copy-start.1
  6.5 0.0 copy-start.4
  6.5 0.0 copy-start.2
  6.5 0.0 copy-start.3
  6.5 0.0 all-reduce.2.cloned.1.call-start
  6.6 1.5 %copy-done = bf16[1024,1024]{1,0:T(8,128)(2,1)S(1)} copy-done((bf16[1024,1024]{1,0:T(8,128)(2,1)S(1)}, bf16[1024,1024]{1,0:T(8,128)(2,1)}, u32[]{:S(2)}) %copy-start) | copy-done | bytes 2097176
  8.1 1.8 %fusion.28 = f32[16,1024]{1,0:T(8,128)} fusion(bf16[1024,1024]{1,0:T(8,128)(2,1)S(1)} %copy-done, bf16[16,1024]{1,0:T(8,128)(2,1)} %param.11, f32[1024]{0:T(1024)} %param.12), kind=kOutput, calls=%fused_computation.41 | convolution fusion | flops 33603584 | bytes 2199552 | tf_op jit(solution)/shard_map/dot_general | solution.py:68
  9.9 0.0 all-reduce.2.cloned.1.call-update
  9.9 0.0 reduce-scatter.2.cloned.1.call-start
  10.0 0.0 copy-done.1
  10.0 0.1 fusion.20
  10.1 0.0 copy-done.4
  10.1 13.5 %psum.15 = f32[16]{0:T(128)S(1)} all-reduce(f32[16]{0:T(128)S(1)} %fusion.20), channel_id=1, replica_groups=mesh['dp'=4,'kv'=4,'tp'=2] {'kv'}, use_global_device_ids=true, to_apply=%region_2.0 | all-reduce | flops 16 | bytes 128 | tf_op jit(solution)/shard_map/psum | solution.py:69
  23.6 0.1 broadcast_compare_fusion
  23.7 1.5 %copy.41 = bf16[16,256,128]{1,2,0:T(8,128)(2,1)S(1)} copy(bf16[16,256,128]{2,1,0:T(8,128)(2,1)} %param.17) | data formatting | bytes 2097152 | tf_op args[6]
  25.2 0.1 multiply_cosine_fusion
  25.3 0.0 copy-done.2
  25.3 0.0 copy-done.3
  25.3 0.1 broadcast_bitcast_fusion
  25.4 0.1 pad_maximum_fusion
  25.5 21.6 %all-reduce.2.cloned.1.call-done = f32[16,1024]{1,0:T(8,128)} async-done(((f32[16,1024]{1,0:T(8,128)}), f32[16,1024]{1,0:T(8,128)}) %all-reduce.2.cloned.1.call-update) | async-done | bytes 65552 | tf_op jit(solution)/shard_map/psum | solution.py:70
  47.1 0.9 broadcast_multiply_fusion
  48.0 0.1 reshape.64
  48.2 0.0 copy-start.5
  48.2 0.1 slice_negate_fusion
  48.3 0.7 fusion.37
  49.0 13.2 %all-gather = f32[64,8,2]{1,2,0:T(2,128)S(1)} all-gather(f32[16,8,2]{1,2,0:T(2,128)S(1)} %get-tuple-element.230), channel_id=2, replica_groups=mesh['dp'=4,'kv'=4,'tp'=2] {'kv'}, dimensions={0}, use_global_device_ids=true | all-gather | bytes 5120 | tf_op jit(solution)/shard_map/all_gather | solution.py:13
  62.1 0.2 fusion.9
  62.4 0.0 copy-done.5
  62.4 0.3 fusion.6
  62.7 15.8 %all-gather.2 = f32[64,8,2,128]{3,1,2,0:T(8,128)S(1)} all-gather(f32[16,8,2,128]{3,1,2,0:T(8,128)S(1)} %fusion.6), channel_id=4, replica_groups=mesh['dp'=4,'kv'=4,'tp'=2] {'kv'}, dimensions={0}, use_global_device_ids=true | all-gather | bytes 655360 | tf_op jit(solution)/shard_map/all_gather | solution.py:13
  78.5 0.1 copy.46
  78.5 13.1 %all-gather.1 = f32[64,8,2]{1,2,0:T(2,128)S(1)} all-gather(f32[16,8,2]{1,2,0:T(2,128)S(1)} %fusion.9), channel_id=3, replica_groups=mesh['dp'=4,'kv'=4,'tp'=2] {'kv'}, dimensions={0}, use_global_device_ids=true | all-gather | bytes 5120 | tf_op jit(solution)/shard_map/all_gather | solution.py:13
  91.7 0.1 copy.48
  91.8 0.1 copy.45
  91.8 0.1 copy.47
  91.9 0.1 copy.44
  92.0 3.4 %while.19 = (s32[]{:T(128)}, f32[16,8,2]{0,2,1:T(2,128)S(1)}, f32[16,8,2]{0,2,1:T(2,128)S(1)}, f32[16,8,2,128]{3,2,1,0:T(2,128)S(1)}, f32[4,16,8,2]{1,3,2,0:T(2,...) while((s32[]{:T(128)}, f32[16,8,2]{0,2,1:T(2,128)S(1)}, ...), condition=%wide.region_6.7_spmd, body=%wide.region_5.6_spmd.sunk | while | flops 99845 | bytes 669847 | solution.py:18
  92.1 0.1 copy.83
  92.2 0.1 copy.84
  92.3 0.8 fusion.44
  93.2 0.1 copy.83
  93.3 0.1 copy.84
  93.5 0.8 fusion.44
  94.3 0.1 copy.83
  94.5 0.1 copy.84
  94.6 0.8 fusion.44
  95.4 0.1 copy.50
  95.5 0.2 broadcast_divide_fusion
  95.8 0.2 slice_reduce_fusion
  96.0 0.2 multiply_reduce_fusion
  96.2 0.1 mul.196
  96.3 2.6 %fusion.26 = f32[16,1024]{1,0:T(8,128)} fusion(bf16[1024,1024]{1,0:T(8,128)(2,1)} %param.16, f32[2,8,8,128]{3,2,1,0:T(8,128)S(1)} %bitcast.72, f32[2,8,8,128]{3,2,1,0:T(8,128)S(1)} %bitcast.71, f32[2,8,8,128]{3,2,1,0:T(8,128)S(1)} %bitcast.68, f32[1024]{0:T(1024)S(1)} %get-tuple-element.234, f32[1024]{0:T(1024)S(1)} %get-tuple-element.235), kind=kOutput, calls=%fused_computation.40 | convolution fusion | flops 33636352 | bytes 2367488 | tf_op jit(solution)/shard_map/dot_general | solution.py:98
  98.9 0.0 reduce-scatter.2.cloned.1.call-update
  98.9 7.8 %reduce-scatter.2.cloned.1.call-done = f32[16,512]{1,0:T(8,128)} async-done(((f32[16,1024]{1,0:T(8,128)}), f32[16,512]{1,0:T(8,128)}) %reduce-scatter.2.cloned.1.call-update) | async-done | bytes 32784 | tf_op jit(solution)/shard_map/reduce_scatter | solution.py:99
  106.6 1.4 %convert_element_type.24 = bf16[16,512]{1,0:T(8,128)(2,1)} convert(f32[16,512]{1,0:T(8,128)} %reduce-scatter.2.cloned.1.call-done) | non-fusion elementwise | flops 8192 | bytes 49152 | tf_op jit(solution)/shard_map/convert_element_type | solution.py:99
  (15 shorter events, 0.2 us)
Async XLA Ops:
  6.5 1.6 %copy-start = (bf16[1024,1024]{1,0:T(8,128)(2,1)S(1)}, bf16[1024,1024]{1,0:T(8,128)(2,1)}, u32[]{:S(2)}) copy-start(bf16[1024,1024]{1,0:T(8,128)(2,1)} %param.13) | copy-start | bytes 6291460
  6.5 3.4 %copy-start.1 = (bf16[16,1024]{1,0:T(8,128)(2,1)S(1)}, bf16[16,1024]{1,0:T(8,128)(2,1)}, u32[]{:S(2)}) copy-start(bf16[16,1024]{1,0:T(8,128)(2,1)} %param.11) | copy-start | bytes 98308
  6.5 3.6 %copy-start.4 = (s32[16]{0:T(128)S(1)}, s32[16]{0:T(128)}, u32[]{:S(2)}) copy-start(s32[16]{0:T(128)} %param.19) | copy-start | bytes 196
  6.5 18.8 %copy-start.2 = (f32[8]{0:T(128)S(1)}, f32[8]{0:T(128)}, u32[]{:S(2)}) copy-start(f32[8]{0:T(128)} %param.14) | copy-start | bytes 100
  6.5 18.8 %copy-start.3 = (f32[128]{0:T(128)S(1)}, f32[128]{0:T(128)}, u32[]{:S(2)}) copy-start(f32[128]{0:T(128)} %param.15) | copy-start | bytes 1540
  6.5 40.6 %all-reduce.2.cloned.1.call-start = ((), (), s32[]{:S(2)}) async-start(), calls=%async_computation.1 | async-start | bytes 131072 | tf_op jit(solution)/shard_map/psum | solution.py:70
  9.9 96.7 %reduce-scatter.2.cloned.1.call-start = ((), (), s32[]{:S(2)}) async-start(), calls=%async_computation.2 | async-start | bytes 98304 | tf_op jit(solution)/shard_map/reduce_scatter | solution.py:99
  48.2 14.2 %copy-start.5 = (bf16[16,256,128]{2,1,0:T(8,128)(2,1)S(1)}, bf16[16,256,128]{2,1,0:T(8,128)(2,1)}, u32[]{:S(2)}) copy-start(bf16[16,256,128]{2,1,0:T(8,128)(2,1)} %param.18) | copy-start | bytes 3145732
Sparse Core Ops, SparseCore 0:
  10.0 37.0 all-reduce.1
  99.0 7.5 reduce-scatter.1
where the time goes:
time: 115 us
  blocking collectives  55.5 us (48%)
  waiting for transfers between devices  29.4 us (26%)
  between operations  13.6 us (12%)
  other arithmetic  5.9 us (5%)
  matrix products  5.38 us (5%)
  local copies, waits for them, and re-layouts  4.94 us (4%)
    all_gather x3, blocking collectives, combined_all(): gathered = jax.tree.map(lambda a: lax.all_gather(a, axis), part)  42 us
    psum x1, waiting for transfers between devices, on_device(): raw_query = lax.psum(partial_query, 'kv')  21.6 us
    psum x1, blocking collectives, on_device(): squares = lax.psum(squares, 'kv')  13.5 us
    reduce_scatter x1, waiting for transfers between devices, on_device(): lax.psum_scatter(projected, 'tp', scatter_dimension=1, tiled=True)  7.75 us
    unnamed x13, local copies, waits for them, and re-layouts  3.04 us
    dot_general x1, matrix products, on_device(): projected = jnp.dot(normed, w_out, preferred_element_type=jnp.float32)  2.61 us
    add x3, other arithmetic, combine_blocks(): earlier[2] * first_factor[..., None] + later[2] * second_factor[..., None]  2.39 us
  transfers between devices with their start and end apart: 2, of which 2 were waited for; matrix products, arithmetic and copies ran while one was open for 2% of the time, Pallas kernels for 0%

commit v1 on v0

--- a/solution.py
+++ b/solution.py
@@ -67,7 +67,7 @@
     scaled_in = (widened * norm_gain).astype(jnp.bfloat16)
     partial_query = jnp.dot(scaled_in, w_query, preferred_element_type=jnp.float32)
     squares = lax.psum(squares, "kv")
-    raw_query = lax.psum(partial_query, "kv")
+    raw_query = jnp.sum(lax.all_gather(partial_query, "kv"), axis=0)
     scale_rows = lax.rsqrt(squares / D + EPS)
     shaped = (raw_query * scale_rows[:, None]).reshape(seq_count, head_count, 2, HEAD_FEATURES)
     query = rotate_query(shaped, (lengths - 1).astype(jnp.float32))

time: 115 us -> 104 us (0.904)
  waiting for transfers between devices: 29.4 us -> 5.95 us
  blocking collectives: 55.5 us -> 69.4 us
    psum x1 -> x0, waiting for transfers between devices: 21.6 us -> none  [on_device(): raw_query = lax.psum(partial_query, 'kv')]
    all_gather x0 -> x1, blocking collectives: none -> 15.6 us  [on_device(): raw_query = jnp.sum(lax.all_gather(partial_query, 'kv'), axis=0)]
    reduce_scatter x1, waiting for transfers between devices: 7.75 us -> 5.93 us  [on_device(): lax.psum_scatter(projected, 'tp', scatter_dimension=1, tiled=True)]
    psum x1, blocking collectives: 13.5 us -> 12.3 us  [on_device(): squares = lax.psum(squares, 'kv')]
    unnamed x13 -> x11, local copies, waits for them, and re-layouts: 3.04 us -> 2.06 us
  transfers between devices with their start and end apart: 2 -> 1, of which waited for: 2 -> 1; matrix products, arithmetic and copies ran while one was open for 2% -> 0% of each run, Pallas kernels for 0% -> 0%
where the time goes in v1:
time: 104 us
  blocking collectives  69.4 us (67%)
  between operations  13.6 us (13%)
  other arithmetic  6.37 us (6%)
  waiting for transfers between devices  5.95 us (6%)
  matrix products  4.68 us (4%)
  local copies, waits for them, and re-layouts  3.95 us (4%)
    all_gather x3, blocking collectives, combined_all(): gathered = jax.tree.map(lambda a: lax.all_gather(a, axis), part)  41.4 us
    all_gather x1, blocking collectives, on_device(): raw_query = jnp.sum(lax.all_gather(partial_query, 'kv'), axis=0)  15.6 us
    psum x1, blocking collectives, on_device(): squares = lax.psum(squares, 'kv')  12.3 us
    reduce_scatter x1, waiting for transfers between devices, on_device(): lax.psum_scatter(projected, 'tp', scatter_dimension=1, tiled=True)  5.93 us
    dot_general x1, matrix products, on_device(): projected = jnp.dot(normed, w_out, preferred_element_type=jnp.float32)  2.61 us
    add x3, other arithmetic, combine_blocks(): earlier[2] * first_factor[..., None] + later[2] * second_factor[..., None]  2.38 us
  transfers between devices with their start and end apart: 1, of which 1 were waited for; matrix products, arithmetic and copies ran while one was open for 0% of the time, Pallas kernels for 0%

profile of v1, /device:TPU:0, one launch (start us, length us, event | category | flops | bytes accessed | tf_op | source)
XLA Modules:
  0.0 103.9 jit_solution(15373554398320479739)
XLA Ops:
  6.5 0.0 copy-start
  6.5 0.0 copy-start.3
  6.5 0.0 reduce-scatter.2.cloned.1.call-start
  6.6 1.0 fusion.17
  7.6 0.6 copy-done
  8.1 1.1 %fusion.23 = f32[16,1024]{1,0:T(8,128)S(1)} fusion(bf16[1024,1024]{1,0:T(8,128)(2,1)S(1)} %copy-done, bf16[16,1024]{1,0:T(8,128)(2,1)} %param.11, f32[1024]{0:T(1024)} %param.12), kind=kOutput, calls=%fused_computation.38 | convolution fusion | flops 33603584 | bytes 2199552 | tf_op jit(solution)/shard_map/dot_general | solution.py:68
  9.3 15.6 %all-gather = f32[64,1024]{1,0:T(8,128)S(1)} all-gather(f32[16,1024]{1,0:T(8,128)S(1)} %fusion.23), channel_id=2, replica_groups=mesh['dp'=4,'kv'=4,'tp'=2] {'kv'}, dimensions={0}, use_global_device_ids=true | all-gather | bytes 327680 | tf_op jit(solution)/shard_map/all_gather | solution.py:70
  25.0 0.1 reduce_sum.39
  25.1 12.3 %psum.7 = f32[16]{0:T(128)S(1)} all-reduce(f32[16]{0:T(128)S(1)} %fusion.17), channel_id=1, replica_groups=mesh['dp'=4,'kv'=4,'tp'=2] {'kv'}, use_global_device_ids=true, to_apply=%region_2.0 | all-reduce | flops 16 | bytes 128 | tf_op jit(solution)/shard_map/psum | solution.py:69
  37.4 0.1 broadcast_multiply_fusion
  37.5 0.2 slice_negate_fusion
  37.7 0.0 copy-done.3
  37.8 0.1 broadcast_compare_fusion
  37.8 1.5 %copy.33 = bf16[16,256,128]{1,2,0:T(8,128)(2,1)S(1)} copy(bf16[16,256,128]{2,1,0:T(8,128)(2,1)} %param.17) | data formatting | bytes 2097152 | tf_op args[6]
  39.3 0.0 copy-start.4
  39.3 0.1 multiply_cosine_fusion
  39.5 0.1 pad_maximum_fusion
  39.5 0.2 fusion.11
  39.8 0.6 fusion.30
  40.4 13.3 %all-gather.1 = f32[64,8,2]{1,2,0:T(2,128)S(1)} all-gather(f32[16,8,2]{1,2,0:T(2,128)S(1)} %get-tuple-element.230), channel_id=3, replica_groups=mesh['dp'=4,'kv'=4,'tp'=2] {'kv'}, dimensions={0}, use_global_device_ids=true | all-gather | bytes 5120 | tf_op jit(solution)/shard_map/all_gather | solution.py:13
  53.7 0.2 fusion.9
  54.0 0.0 copy-done.4
  54.0 0.3 fusion.6
  54.3 14.9 %all-gather.3 = f32[64,8,2,128]{3,1,2,0:T(8,128)S(1)} all-gather(f32[16,8,2,128]{3,1,2,0:T(8,128)S(1)} %fusion.6), channel_id=5, replica_groups=mesh['dp'=4,'kv'=4,'tp'=2] {'kv'}, dimensions={0}, use_global_device_ids=true | all-gather | bytes 655360 | tf_op jit(solution)/shard_map/all_gather | solution.py:13
  69.2 0.1 copy.39
  69.3 13.1 %all-gather.2 = f32[64,8,2]{1,2,0:T(2,128)S(1)} all-gather(f32[16,8,2]{1,2,0:T(2,128)S(1)} %fusion.9), channel_id=4, replica_groups=mesh['dp'=4,'kv'=4,'tp'=2] {'kv'}, dimensions={0}, use_global_device_ids=true | all-gather | bytes 5120 | tf_op jit(solution)/shard_map/all_gather | solution.py:13
  82.4 0.1 copy.41
  82.5 0.1 copy.38
  82.6 0.1 copy.40
  82.7 0.1 copy.37
  82.8 0.0 copy-start.1
  82.8 0.0 copy-start.2
  82.8 3.4 %while.19 = (s32[]{:T(128)}, f32[16,8,2]{0,2,1:T(2,128)S(1)}, f32[16,8,2]{0,2,1:T(2,128)S(1)}, f32[16,8,2,128]{3,2,1,0:T(2,128)S(1)}, f32[4,16,8,2]{1,3,2,0:T(2,...) while((s32[]{:T(128)}, f32[16,8,2]{0,2,1:T(2,128)S(1)}, ...), condition=%wide.region_6.7_spmd, body=%wide.region_5.6_spmd.sunk | while | flops 99845 | bytes 669847 | solution.py:18
  82.8 0.1 copy.74
  83.0 0.1 copy.75
  83.1 0.8 fusion.37
  84.0 0.1 copy.74
  84.1 0.1 copy.75
  84.3 0.8 fusion.37
  85.1 0.1 copy.74
  85.2 0.1 copy.75
  85.4 0.8 fusion.37
  86.2 0.1 copy.43
  86.3 0.2 broadcast_divide_fusion
  86.5 0.2 slice_reduce_fusion
  86.8 0.0 copy-done.1
  86.8 0.2 multiply_reduce_fusion
  87.0 0.0 copy-done.2
  87.0 0.1 broadcast_bitcast_fusion
  87.1 0.1 mul.197
  87.1 2.6 %fusion.21 = f32[16,1024]{1,0:T(8,128)} fusion(bf16[1024,1024]{1,0:T(8,128)(2,1)} %param.16, f32[2,8,8,128]{3,2,1,0:T(8,128)S(1)} %bitcast.74, f32[2,8,8,128]{3,2,1,0:T(8,128)S(1)} %bitcast.73, f32[2,8,8,128]{3,2,1,0:T(8,128)S(1)} %bitcast.70, f32[1024]{0:T(1024)S(1)} %get-tuple-element.234, f32[1024]{0:T(1024)S(1)} %get-tuple-element.235), kind=kOutput, calls=%fused_computation.37 | convolution fusion | flops 33636352 | bytes 2367488 | tf_op jit(solution)/shard_map/dot_general | solution.py:98
  89.7 0.0 reduce-scatter.2.cloned.1.call-update
  89.8 5.9 %reduce-scatter.2.cloned.1.call-done = f32[16,512]{1,0:T(8,128)} async-done(((f32[16,1024]{1,0:T(8,128)}), f32[16,512]{1,0:T(8,128)}) %reduce-scatter.2.cloned.1.call-update) | async-done | bytes 32784 | tf_op jit(solution)/shard_map/reduce_scatter | solution.py:99
  95.7 1.4 %convert_element_type.24 = bf16[16,512]{1,0:T(8,128)(2,1)} convert(f32[16,512]{1,0:T(8,128)} %reduce-scatter.2.cloned.1.call-done) | non-fusion elementwise | flops 8192 | bytes 49152 | tf_op jit(solution)/shard_map/convert_element_type | solution.py:99
  (15 shorter events, 0.2 us)
Async XLA Ops:
  6.5 1.6 %copy-start = (bf16[1024,1024]{1,0:T(8,128)(2,1)S(1)}, bf16[1024,1024]{1,0:T(8,128)(2,1)}, u32[]{:S(2)}) copy-start(bf16[1024,1024]{1,0:T(8,128)(2,1)} %param.13) | copy-start | bytes 6291460
  6.5 31.2 %copy-start.3 = (s32[16]{0:T(128)S(1)}, s32[16]{0:T(128)}, u32[]{:S(2)}) copy-start(s32[16]{0:T(128)} %param.19) | copy-start | bytes 196
  6.5 89.2 %reduce-scatter.2.cloned.1.call-start = ((), (), s32[]{:S(2)}) async-start(), calls=%async_computation.1 | async-start | bytes 98304 | tf_op jit(solution)/shard_map/reduce_scatter | solution.py:99
  39.3 14.6 %copy-start.4 = (bf16[16,256,128]{2,1,0:T(8,128)(2,1)S(1)}, bf16[16,256,128]{2,1,0:T(8,128)(2,1)}, u32[]{:S(2)}) copy-start(bf16[16,256,128]{2,1,0:T(8,128)(2,1)} %param.18) | copy-start | bytes 3145732
  82.8 4.0 %copy-start.1 = (f32[8]{0:T(128)S(1)}, f32[8]{0:T(128)}, u32[]{:S(2)}) copy-start(f32[8]{0:T(128)} %param.14) | copy-start | bytes 100
  82.8 4.2 %copy-start.2 = (f32[128]{0:T(128)S(1)}, f32[128]{0:T(128)}, u32[]{:S(2)}) copy-start(f32[128]{0:T(128)} %param.15) | copy-start | bytes 1540
Sparse Core Ops, SparseCore 0:
  89.9 5.7 reduce-scatter.1
